TPU v7x, 256 devices: a whole 4x4x8 slice. The times are simulated.
256 devices in a mesh: ep: 16 (over y, x), tp: 16 (over z, core).
Axes of the slice: x: 4, y: 4, z: 8, core: 2. Of those that a mesh axis runs over, the one named last changes fastest.
Arguments:
- layer_in: bfloat16 [512, 2048], P('ep'), may hold values from -6 to 6
- attn_gain: float32 [2048], replicated, may hold values from 0.1 to 1.9
- query_weight: bfloat16 [2048, 1024], P(None, 'tp'), may hold values from -0.125 to 0.125
- key_weight: bfloat16 [2048, 1024], P(None, 'tp'), may hold values from -0.125 to 0.125
- value_weight: bfloat16 [2048, 1024], P(None, 'tp'), may hold values from -0.125 to 0.125
- forget_weight: bfloat16 [2048, 16], replicated, may hold values from -0.125 to 0.125
- forget_bias: float32 [16], replicated, may hold values from -2 to 3
- out_weight: bfloat16 [1024, 2048], P('tp'), may hold values from -0.1875 to 0.1875
- kv_cache: bfloat16 [512, 16, 1024, 128], P('ep', 'tp'), may hold values from -110 to 110
- cum_gates: float32 [512, 16, 1024], P('ep', 'tp'), may hold values from -144 to 0, as said below
- lengths: int32 [512], P('ep'), may hold values from 512 to 1024, as said below
- ffn_gain: float32 [2048], replicated, may hold values from 0.1 to 1.9
- route_ids: int32 [512, 6], P('ep'), may hold values from 0 to 127, all different within a row; in each aligned block of 32 rows (0 to 31, 32 to 63, ...) at most 2 rows name the same one
- route_weights: float32 [512, 6], P('ep'), may hold values from 0.1 to 1
- shared_gate: bfloat16 [2048, 512], P(None, 'tp'), may hold values from -0.125 to 0.125
- shared_up: bfloat16 [2048, 512], P(None, 'tp'), may hold values from -0.125 to 0.125
- shared_down: bfloat16 [512, 2048], P('tp'), may hold values from -0.25 to 0.25
- expert_gate: bfloat16 [256, 2048, 256], P(('ep', 'tp')), may hold values from -0.125 to 0.125
- expert_up: bfloat16 [256, 2048, 256], P(('ep', 'tp')), may hold values from -0.125 to 0.125
- expert_down: bfloat16 [256, 256, 2048], P(('ep', 'tp')), may hold values from -0.25 to 0.25
Outputs:
- layer_out: bfloat16 [512, 2048], P('ep')
- new_kv: bfloat16 [512, 16, 128], P('ep', 'tp')
Inputs may be any that keep to these rules, and one draw needn't show every extreme that they name: `cum_gates`: never rising along positions. `lengths`: every length is at most 1024, and some sequence's length is exactly 1024. `route_ids`: each row names 6 different experts. Among the 32 rows of one index of ep (aligned blocks), no expert is named by more than 2 rows, and in some block one expert is named by exactly 2 rows.
All inputs are finite; a program needn't handle non-finite values.
Results may differ from a plain program's by a relative error of at most 0.019.
Values may be sent and summed in bfloat16 or wider, within the bound.
A program may use at most 64 MiB of HBM per device.

v0:
```python
import jax
import jax.numpy as jnp
from jax import lax
from jax.sharding import PartitionSpec as P

NORM_EPS = 1e-06


def cut_along(shard, dim, peers):
    before, after = (shard.shape[:dim], shard.shape[dim + 1 :])
    return jnp.moveaxis(shard.reshape(*before, peers, -1, *after), dim, 0)


def summed_on_arrival(shard, axis, dim):
    tiles = cut_along(shard, dim, lax.axis_size(axis))
    arrived = lax.all_to_all(tiles, axis, split_axis=0, concat_axis=0, tiled=True)
    return arrived.astype(jnp.float32).sum(axis=0)


def in_one_piece(arrays, axis, dim, along):
    both = jnp.concatenate(arrays, axis=along)
    filled, at, outs = (lax.all_gather(both, axis, axis=dim, tiled=True), 0, [])
    for a in arrays:
        outs.append(lax.slice_in_dim(filled, at, at + a.shape[along], axis=along))
        at += a.shape[along]
    return tuple(outs)


def rms_scale(stream, gain):
    wide = stream.astype(jnp.float32)
    factor = lax.rsqrt(jnp.mean(wide * wide, axis=-1, keepdims=True) + NORM_EPS)
    return (wide * factor * gain).astype(jnp.bfloat16)


def project(normed, weight):
    return jnp.dot(normed, weight, preferred_element_type=jnp.float32).astype(jnp.bfloat16)


def attend(queries, new_key, new_value, forget, kv_block, cum_block, length_block):
    head_size = queries.shape[-1]
    cache_span = kv_block.shape[2]
    positions = jnp.arange(cache_span, dtype=jnp.int32)
    inside = positions[None, None, :] < length_block[:, None, None]
    at_last = positions[None, None, :] == (length_block - 1)[:, None, None]
    latest = jnp.sum(jnp.where(at_last, cum_block, 0.0), axis=-1)
    scaling = head_size ** (-0.5)
    cached_keys = kv_block[..., :head_size]
    cached_values = kv_block[..., head_size:]
    scores = (
        jnp.einsum("shd,shld->shl", queries, cached_keys, preferred_element_type=jnp.float32)
        * scaling
    )
    scores = jnp.where(inside, scores + (latest + forget)[..., None] - cum_block, -jnp.inf)
    itself = jnp.sum(queries.astype(jnp.float32) * new_key.astype(jnp.float32), axis=-1) * scaling
    highest = jnp.maximum(jnp.max(scores, axis=-1), itself)
    earlier = jnp.exp(scores - highest[..., None])
    own_term = jnp.exp(itself - highest)
    denominator = jnp.sum(earlier, axis=-1) + own_term
    past_probs = (earlier / denominator[..., None]).astype(jnp.bfloat16)
    own_probs = (own_term / denominator).astype(jnp.bfloat16)
    blended = jnp.einsum(
        "shl,shld->shd", past_probs, cached_values, preferred_element_type=jnp.float32
    )
    blended = blended + own_probs.astype(jnp.float32)[..., None] * new_value.astype(jnp.float32)
    return blended.astype(jnp.bfloat16)


def body(
    layer_in,
    attn_gain,
    query_weight,
    key_weight,
    value_weight,
    forget_weight,
    forget_bias,
    out_weight,
    kv_cache,
    cum_gates,
    lengths,
    ffn_gain,
    route_ids,
    route_weights,
    shared_gate,
    shared_up,
    shared_down,
    expert_gate,
    expert_up,
    expert_down,
):
    row_count = layer_in.shape[0]
    width = layer_in.shape[1]
    heads_here = kv_cache.shape[1]
    head_size = kv_cache.shape[3] // 2
    normed = rms_scale(layer_in, attn_gain)
    queries = project(normed, query_weight).reshape(row_count, heads_here, head_size)
    new_key = project(normed, key_weight).reshape(row_count, heads_here, head_size)
    new_value = project(normed, value_weight).reshape(row_count, heads_here, head_size)
    new_kv = jnp.concatenate([new_key, new_value], axis=-1)
    first_head = lax.axis_index("tp") * heads_here
    gate_logits = jnp.dot(normed, forget_weight, preferred_element_type=jnp.float32) + forget_bias
    forget = jax.nn.log_sigmoid(lax.dynamic_slice_in_dim(gate_logits, first_head, heads_here, 1))
    attended = attend(queries, new_key, new_value, forget, kv_cache, cum_gates, lengths)
    head_part = jnp.dot(
        attended.reshape(row_count, heads_here * head_size),
        out_weight,
        preferred_element_type=jnp.float32,
    )
    slice_rows = row_count // lax.axis_size("tp")
    slice_start = lax.axis_index("tp") * slice_rows
    head_slice = summed_on_arrival(head_part.astype(jnp.bfloat16), "tp", 0)
    own_stream = lax.dynamic_slice_in_dim(layer_in, slice_start, slice_rows, 0)
    middle_slice = (own_stream.astype(jnp.float32) + head_slice).astype(jnp.bfloat16)
    hidden_slice = rms_scale(middle_slice, ffn_gain)
    middle, hidden_in = in_one_piece((middle_slice, hidden_slice), "tp", 0, 1)
    shared_hidden = (
        jax.nn.silu(jnp.dot(hidden_in, shared_gate, preferred_element_type=jnp.float32))
        * jnp.dot(hidden_in, shared_up, preferred_element_type=jnp.float32)
    ).astype(jnp.bfloat16)
    shared_part = jnp.dot(shared_hidden, shared_down, preferred_element_type=jnp.float32)
    my_gate = expert_gate[0]
    my_up = expert_up[0]
    my_down = expert_down[0]
    ep_count = lax.axis_size("ep")
    pair_count = lax.axis_size("tp") // 2
    column = lax.axis_index("tp") // 2
    picks = route_ids.shape[1]
    experts = ep_count * pair_count
    capacity = max(2, 4 * row_count * picks // (3 * experts))
    targets = jnp.arange(ep_count, dtype=jnp.int32) * pair_count + column
    matches = route_ids[:, :, None] == targets[None, None, :]
    member = jnp.any(matches, axis=1).astype(jnp.int32)
    weight = jnp.sum(jnp.where(matches, route_weights[:, :, None], 0.0), axis=1)
    ranking = jnp.cumsum(member, axis=0) - member
    slot_numbers = jnp.arange(capacity, dtype=jnp.int32)
    placement = (member[:, :, None] == 1) & (ranking[:, :, None] == slot_numbers[None, None, :])
    dispatch = jnp.einsum(
        "rs,rd->sd",
        placement.reshape(row_count, ep_count * capacity).astype(jnp.bfloat16),
        hidden_in,
        preferred_element_type=jnp.float32,
    ).astype(jnp.bfloat16)
    dispatch = dispatch.reshape(ep_count, capacity, width)
    received = lax.all_to_all(dispatch, "ep", split_axis=0, concat_axis=0, tiled=True)
    count = received.shape[1]
    batch_rows = received.reshape(ep_count * count, width)
    hidden = (
        jax.nn.silu(jnp.dot(batch_rows, my_gate, preferred_element_type=jnp.float32))
        * jnp.dot(batch_rows, my_up, preferred_element_type=jnp.float32)
    ).astype(jnp.bfloat16)
    served = jnp.dot(hidden, my_down, preferred_element_type=jnp.float32).reshape(
        ep_count, count, width
    )
    returned = lax.all_to_all(
        served.astype(jnp.bfloat16), "ep", split_axis=0, concat_axis=0, tiled=True
    ).astype(served.dtype)
    shares = (placement.astype(jnp.float32) * weight[:, :, None]).reshape(
        row_count, ep_count * capacity
    )
    routed = jnp.dot(
        shares,
        returned.reshape(ep_count * capacity, width),
        precision=lax.Precision.HIGHEST,
        preferred_element_type=jnp.float32,
    )
    mixed_slice = summed_on_arrival((shared_part + routed).astype(jnp.bfloat16), "tp", 0)
    own_middle = lax.dynamic_slice_in_dim(middle, slice_start, slice_rows, 0)
    out_slice = (own_middle.astype(jnp.float32) + mixed_slice).astype(jnp.bfloat16)
    layer_out = lax.all_gather(out_slice, "tp", axis=0, tiled=True)
    return (layer_out, new_kv)


def solution(mesh):
    placed = (
        P("ep", None),
        P(),
        P(None, "tp"),
        P(None, "tp"),
        P(None, "tp"),
        P(),
        P(),
        P("tp", None),
        P("ep", "tp", None, None),
        P("ep", "tp", None),
        P("ep"),
        P(),
        P("ep", None),
        P("ep", None),
        P(None, "tp"),
        P(None, "tp"),
        P("tp", None),
        P(("ep", "tp"), None, None),
        P(("ep", "tp"), None, None),
        P(("ep", "tp"), None, None),
    )
    return jax.shard_map(
        body,
        mesh=mesh,
        in_specs=placed,
        out_specs=(P("ep", None), P("ep", "tp", None)),
        check_vma=False,
    )
```

profile of v0, /device:TPU:1, one launch (start us, length us, event | category | flops | bytes accessed | tf_op | source)
XLA Modules:
  0.0 121.0 jit_solution(8280109137043809349)
XLA Ops:
  0.7 1.1 fusion.13
  2.5 1.1 fusion.55
  3.7 1.3 %convolution_convert_fusion.5 = bf16[32,64]{1,0:T(8,128)(2,1)S(1)} fusion(bf16[2048,64]{0,1:T(8,128)(2,1)} %param.22, bf16[32,2048]{1,0:T(8,128)(2,1)} %param.20, f32[2048]{0:T(1024)} %param.21, f32[32]{0:T(128)S(1)} %add_rsqrt_fusion.1), kind=kOutput, calls=%fused_computation.18 | convolution fusion | flops 8652800 | bytes 405632 | tf_op jit(solution)/shard_map/dot_general | solution.py:36
  5.0 1.4 %dynamic-slice = f32[1]{0:T(128)} dynamic-slice(f32[16]{0:T(128)} %param.26, s32[]{:T(128)S(6)} %select_n.30), dynamic_slice_sizes={1} | dynamic-slice | bytes 12 | tf_op jit(solution)/shard_map/dynamic_slice | solution.py:101
  6.4 1.8 %fusion.21 = f32[32]{0:T(128)S(1)} fusion(f32[32,1,1024]{2,1,0:T(1,128)} %param.29, s32[32]{0:T(128)S(1)} %broadcast_add_fusion), kind=kLoop, calls=%fused_computation.39 | loop fusion | flops 98272 | bytes 131328 | tf_op jit(solution)/shard_map/reduce_sum | solution.py:45
  8.1 5.6 %fusion.2 = f32[32,1,1024]{2,1,0:T(1,128)S(1)} fusion(bf16[32,1,1024,128]{3,2,1,0:T(8,128)(2,1)} %param.28, bf16[32,64,1]{1,0,2:T(8,128)(2,1)S(1)} %bitcast.54), kind=kOutput, calls=%fused_computation.2 | convolution fusion | flops 4194304 | bytes 8523776 | tf_op jit(solution)/shard_map/shd,shld->shl/dot_general | solution.py:50
  15.2 1.0 multiply_reduce_fusion
  16.8 2.6 %fusion = f32[32,1,64]{2,1,0:T(1,128)S(1)} fusion(bf16[32,1,1024,128]{3,2,1,0:T(8,128)(2,1)S(1)} %copy-done.1, f32[32]{0:T(128)S(1)} %get-tuple-element.9, f32[32,1,1024]{2,1,0:T(1,128)S(1)} %get-tuple-element.5, f32[32]{0:T(128)S(1)} %multiply_maximum_fusion), kind=kOutput, calls=%fused_computation | convolution fusion | flops 4292608 | bytes 8528128 | tf_op jit(solution)/shard_map/shl,shld->shd/dot_general | solution.py:61
  20.7 10.0 %all-to-all-start = ((bf16[16,2,2048]{2,1,0:T(2,128)(2,1)}), bf16[16,2,2048]{2,1,0:T(2,128)(2,1)S(1)}, u32[]{:S(2)}, u32[]{:S(2)}) async-start(bf16[16,2,2048]{2,1,0:T(2,128)(2,1)} %reshape.219), calls=%async_computation | async-start | bytes 262144 | tf_op jit(solution)/shard_map/all_to_all | solution.py:16
  33.1 6.5 %all-to-all-done = bf16[16,2,2048]{2,1,0:T(2,128)(2,1)S(1)} async-done(((bf16[16,2,2048]{2,1,0:T(2,128)(2,1)}), bf16[16,2,2048]{2,1,0:T(2,128)(2,1)S(1)}, u32[]{:S(2)}, u32[]{:S(2)}) %all-to-all-start) | async-done | bytes 131104 | tf_op jit(solution)/shard_map/all_to_all | solution.py:16
  39.9 16.6 %all-gather = bf16[16,2,4096]{2,1,0:T(2,128)(2,1)} all-gather(bf16[1,2,4096]{2,1,0:T(2,128)(2,1)S(1)} %maximum_bitcast_fusion), channel_id=1, replica_groups=mesh['ep'=16,'tp'=16] {'tp'}, dimensions={0}, use_global_device_ids=true | all-gather | bytes 278528 | tf_op jit(solution)/shard_map/all_gather | solution.py:22
  56.5 1.0 reshape.226
  59.2 6.8 %all-to-all-start.1 = ((bf16[16,2,2048]{2,1,0:T(2,128)(2,1)}), bf16[16,2,2048]{2,1,0:T(2,128)(2,1)}, u32[]{:S(2)}, u32[]{:S(2)}) async-start(bf16[16,2,2048]{2,1,0:T(2,128)(2,1)} %reshape.220), calls=%async_computation.1 | async-start | bytes 262144 | tf_op jit(solution)/shard_map/all_to_all | solution.py:143
  66.0 1.3 %and_select_fusion = f32[32,16,2]{0,2,1:T(2,128)} fusion(pred[32,16]{0,1:T(8,128)(4,1)} %copy-done.7, f32[32,16]{0,1:T(8,128)} %fusion.28, s32[32,16]{0,1:T(8,128)S(1)} %copy.41), kind=kLoop, calls=%fused_computation.48 | loop fusion | flops 3072 | bytes 8704 | tf_op jit(solution)/shard_map/mul | solution.py:156
  67.4 5.6 %all-to-all-done.1 = bf16[16,2,2048]{2,1,0:T(2,128)(2,1)} async-done(((bf16[16,2,2048]{2,1,0:T(2,128)(2,1)}), bf16[16,2,2048]{2,1,0:T(2,128)(2,1)}, u32[]{:S(2)}, u32[]{:S(2)}) %all-to-all-start.1) | async-done | bytes 131104 | tf_op jit(solution)/shard_map/all_to_all | solution.py:143
  75.6 3.5 %all-to-all-start.2 = ((bf16[16,2,2048]{2,1,0:T(2,128)(2,1)}), bf16[16,2,2048]{2,1,0:T(2,128)(2,1)S(1)}, u32[]{:S(2)}, u32[]{:S(2)}) async-start(bf16[16,2,2048]{2,1,0:T(2,128)(2,1)} %copy.43), calls=%async_computation.2 | async-start | bytes 262144 | tf_op jit(solution)/shard_map/all_to_all | solution.py:153
  79.1 1.1 fusion.25
  80.2 5.7 %all-to-all-done.2 = bf16[16,2,2048]{2,1,0:T(2,128)(2,1)S(1)} async-done(((bf16[16,2,2048]{2,1,0:T(2,128)(2,1)}), bf16[16,2,2048]{2,1,0:T(2,128)(2,1)S(1)}, u32[]{:S(2)}, u32[]{:S(2)}) %all-to-all-start.2) | async-done | bytes 131104 | tf_op jit(solution)/shard_map/all_to_all | solution.py:153
  85.9 1.0 convolution_bitcast_fusion
  87.0 1.3 %fusion.6 = bf16[32,2048]{1,0:T(8,128)(2,1)S(1)} fusion(f32[32,2048]{1,0:T(8,128)S(1)} %convolution_bitcast_fusion, bf16[32,2048]{1,0:T(8,128)(2,1)} %param.36, bf16[2048,32]{0,1:T(8,128)(2,1)} %param.35, bf16[32,4096]{1,0:T(8,128)(2,1)S(1)} %reshape.226, f32[32,32]{1,0:T(8,128)S(1)} %fusion.25), kind=kOutput, calls=%fused_computation.8 | convolution fusion | flops 8525824 | bytes 802816 | tf_op jit(solution)/shard_map/dot_general | solution.py:119
  89.1 7.4 %all-to-all-start.3 = ((bf16[16,2,2048]{2,1,0:T(2,128)(2,1)}), bf16[16,2,2048]{2,1,0:T(2,128)(2,1)S(1)}, u32[]{:S(2)}, u32[]{:S(2)}) async-start(bf16[16,2,2048]{2,1,0:T(2,128)(2,1)} %reshape.222), calls=%async_computation.3 | async-start | bytes 262144 | tf_op jit(solution)/shard_map/all_to_all | solution.py:16
  96.5 1.4 %pad_maximum_fusion = bf16[32,1,128]{2,0,1:T(8,128)(2,1)} fusion(bf16[32,1,64]{2,0,1:T(8,128)(2,1)S(1)} %bitcast.55, bf16[32,1,64]{2,0,1:T(8,128)(2,1)} %bitcast.57), kind=kLoop, calls=%fused_computation.72 | loop fusion | flops 16384 | bytes 16384 | tf_op jit(solution)/shard_map/concatenate | solution.py:98
  97.9 7.5 %all-to-all-done.3 = bf16[16,2,2048]{2,1,0:T(2,128)(2,1)S(1)} async-done(((bf16[16,2,2048]{2,1,0:T(2,128)(2,1)}), bf16[16,2,2048]{2,1,0:T(2,128)(2,1)S(1)}, u32[]{:S(2)}, u32[]{:S(2)}) %all-to-all-start.3) | async-done | bytes 131104 | tf_op jit(solution)/shard_map/all_to_all | solution.py:16
  105.5 14.8 %all-gather.1 = bf16[16,2,2048]{2,1,0:T(2,128)(2,1)S(1)} all-gather(bf16[1,2,2048]{2,1,0:T(2,128)(2,1)S(1)} %fusion.42), channel_id=1, replica_groups=mesh['ep'=16,'tp'=16] {'tp'}, dimensions={0}, use_global_device_ids=true | all-gather | bytes 139264 | tf_op jit(solution)/shard_map/all_gather | solution.py:168
  (73 shorter events, 12.6 us)
Async XLA Ops:
  0.6 73.9 %copy-start = (bf16[1,256,2048]{2,1,0:T(8,128)(2,1)S(1)}, bf16[1,256,2048]{2,1,0:T(8,128)(2,1)}, u32[]{:S(2)}) copy-start(bf16[1,256,2048]{2,1,0:T(8,128)(2,1)} %param.39) | copy-start | bytes 3145732
  0.6 14.6 %copy-start.6 = (bf16[32,2048]{1,0:T(8,128)(2,1)S(1)}, bf16[32,2048]{1,0:T(8,128)(2,1)}, u32[]{:S(2)}) copy-start(bf16[32,2048]{1,0:T(8,128)(2,1)} %param.20) | copy-start | bytes 393220
  0.7 14.0 %copy-start.11 = (s32[32]{0:T(128)S(1)}, s32[32]{0:T(128)}, u32[]{:S(2)}) copy-start(s32[32]{0:T(128)} %param.30) | copy-start | bytes 388
  0.7 14.5 %copy-start.14 = (f32[2048]{0:T(1024)S(1)}, f32[2048]{0:T(1024)}, u32[]{:S(2)}) copy-start(f32[2048]{0:T(1024)} %param.21) | copy-start | bytes 24580
  0.7 14.0 %copy-start.4 = (f32[32,1,1024]{2,1,0:T(1,128)S(1)}, f32[32,1,1024]{2,1,0:T(1,128)}, u32[]{:S(2)}) copy-start(f32[32,1,1024]{2,1,0:T(1,128)} %param.29) | copy-start | bytes 393220
  0.7 14.5 %copy-start.12 = (bf16[2048,64]{0,1:T(8,128)(2,1)S(1)}, bf16[2048,64]{0,1:T(8,128)(2,1)}, u32[]{:S(2)}) copy-start(bf16[2048,64]{0,1:T(8,128)(2,1)} %param.23) | copy-start | bytes 786436
  5.0 11.8 %copy-start.1 = (bf16[32,1,1024,128]{3,2,1,0:T(8,128)(2,1)S(1)}, bf16[32,1,1024,128]{3,2,1,0:T(8,128)(2,1)}, u32[]{:S(2)}) copy-start(bf16[32,1,1024,128]{3,2,1,0:T(8,128)(2,1)} %param.28) | copy-start | bytes 25165828
  13.8 5.6 %copy-start.13 = (bf16[2048,64]{0,1:T(8,128)(2,1)S(1)}, bf16[2048,64]{0,1:T(8,128)(2,1)}, u32[]{:S(2)}) copy-start(bf16[2048,64]{0,1:T(8,128)(2,1)} %param.24) | copy-start | bytes 786436
  13.8 5.9 %copy-start.5 = (bf16[64,2048]{1,0:T(8,128)(2,1)S(1)}, bf16[64,2048]{1,0:T(8,128)(2,1)}, u32[]{:S(2)}) copy-start(bf16[64,2048]{1,0:T(8,128)(2,1)} %param.27) | copy-start | bytes 786436
  13.8 16.9 %copy-start.8 = (s32[32,6]{0,1:T(8,128)S(1)}, s32[32,6]{0,1:T(8,128)}, u32[]{:S(2)}) copy-start(s32[32,6]{0,1:T(8,128)} %param.32) | copy-start | bytes 2308
  13.8 18.6 %copy-start.10 = (f32[32,6]{0,1:T(8,128)S(1)}, f32[32,6]{0,1:T(8,128)}, u32[]{:S(2)}) copy-start(f32[32,6]{0,1:T(8,128)} %param.33) | copy-start | bytes 2308
  13.8 26.0 %copy-start.9 = (f32[2048]{0:T(1024)S(1)}, f32[2048]{0:T(1024)}, u32[]{:S(2)}) copy-start(f32[2048]{0:T(1024)} %param.31) | copy-start | bytes 24580
  15.2 58.7 %copy-start.2 = (bf16[1,2048,256]{2,1,0:T(8,128)(2,1)S(1)}, bf16[1,2048,256]{2,1,0:T(8,128)(2,1)}, u32[]{:S(2)}) copy-start(bf16[1,2048,256]{2,1,0:T(8,128)(2,1)} %param.37) | copy-start | bytes 3145732
  16.8 57.4 %copy-start.3 = (bf16[1,2048,256]{2,1,0:T(8,128)(2,1)S(1)}, bf16[1,2048,256]{2,1,0:T(8,128)(2,1)}, u32[]{:S(2)}) copy-start(bf16[1,2048,256]{2,1,0:T(8,128)(2,1)} %param.38) | copy-start | bytes 3145732
  20.7 18.9 %all-to-all-start = ((bf16[16,2,2048]{2,1,0:T(2,128)(2,1)}), bf16[16,2,2048]{2,1,0:T(2,128)(2,1)S(1)}, u32[]{:S(2)}, u32[]{:S(2)}) async-start(bf16[16,2,2048]{2,1,0:T(2,128)(2,1)} %reshape.219), calls=%async_computation | async-start | bytes 262144 | tf_op jit(solution)/shard_map/all_to_all | solution.py:16
  31.1 2.0 %copy-start.7 = (pred[32,16]{0,1:T(8,128)(4,1)}, pred[32,16]{0,1:T(8,128)(4,1)S(1)}, u32[]{:S(2)}) copy-start(pred[32,16]{0,1:T(8,128)(4,1)S(1)} %copy.40) | copy-start | bytes 1540
  59.2 13.7 %all-to-all-start.1 = ((bf16[16,2,2048]{2,1,0:T(2,128)(2,1)}), bf16[16,2,2048]{2,1,0:T(2,128)(2,1)}, u32[]{:S(2)}, u32[]{:S(2)}) async-start(bf16[16,2,2048]{2,1,0:T(2,128)(2,1)} %reshape.220), calls=%async_computation.1 | async-start | bytes 262144 | tf_op jit(solution)/shard_map/all_to_all | solution.py:143
  75.6 10.3 %all-to-all-start.2 = ((bf16[16,2,2048]{2,1,0:T(2,128)(2,1)}), bf16[16,2,2048]{2,1,0:T(2,128)(2,1)S(1)}, u32[]{:S(2)}, u32[]{:S(2)}) async-start(bf16[16,2,2048]{2,1,0:T(2,128)(2,1)} %copy.43), calls=%async_computation.2 | async-start | bytes 262144 | tf_op jit(solution)/shard_map/all_to_all | solution.py:153
  89.1 16.3 %all-to-all-start.3 = ((bf16[16,2,2048]{2,1,0:T(2,128)(2,1)}), bf16[16,2,2048]{2,1,0:T(2,128)(2,1)S(1)}, u32[]{:S(2)}, u32[]{:S(2)}) async-start(bf16[16,2,2048]{2,1,0:T(2,128)(2,1)} %reshape.222), calls=%async_computation.3 | async-start | bytes 262144 | tf_op jit(solution)/shard_map/all_to_all | solution.py:16
where the time goes:
time: 122 us; the launch traced here: 121 us
  blocking collectives  31.4 us (26%)
  starting transfers between devices  27.7 us (23%)
  waiting for transfers between devices  25.3 us (21%)
  matrix products  17.3 us (14%)
  other arithmetic  9.49 us (8%)
  local copies, waits for them, and re-layouts  8.9 us (7%)
    all_to_all x2, starting transfers between devices, summed_on_arrival(): lax.all_to_all(tiles, axis, split_axis=0, concat_axis=0, tiled=True)  17.4 us
    all_gather x1, blocking collectives, in_one_piece(): filled, at, outs = (lax.all_gather(both, axis, axis=dim, tiled=True), 0, [])  16.6 us
    all_gather x1, blocking collectives, body(): layer_out = lax.all_gather(out_slice, 'tp', axis=0, tiled=True)  14.8 us
    all_to_all x2, waiting for transfers between devices, summed_on_arrival(): lax.all_to_all(tiles, axis, split_axis=0, concat_axis=0, tiled=True)  14 us
    all_to_all x1, starting transfers between devices, body(): lax.all_to_all(dispatch, 'ep', split_axis=0, concat_axis=0, tiled=True)  6.8 us
    all_to_all x1, waiting for transfers between devices, body(): lax.all_to_all(served.astype(jnp.bfloat16), 'ep', split_axis=0, concat_ax...  5.74 us
    dot_general x1, matrix products, attend(): jnp.einsum('shd,shld->shl', queries, cached_keys, preferred_element_type=...  5.63 us
    all_to_all x1, waiting for transfers between devices, body(): lax.all_to_all(dispatch, 'ep', split_axis=0, concat_axis=0, tiled=True)  5.58 us
  transfers between devices with their start and end apart: 4, of which 4 were waited for; matrix products, arithmetic and copies ran while one was open for 5% of the time, Pallas kernels for 0%

commit v1 on v0

v1 whole, which is shorter than its diff:
```python
import jax
import jax.numpy as jnp
from jax import lax
from jax.experimental import pallas as pl
from jax.experimental.pallas import tpu as pltpu
from jax.sharding import PartitionSpec as P

NORM_EPS = 1e-06
MESH = pl.DeviceIdType.MESH
BF = jnp.bfloat16
F32 = jnp.float32
N = 16
ROWS = 32
WIDTH = 2048
LANES = 128
SPAN = 1024
HEAD = 64
TP_ORDER = (8, 9, 7, 6, 10, 11, 5, 4, 12, 13, 3, 2, 14, 15, 1)
EP_ORDER = (10, 6, 14, 9, 11, 2, 8, 5, 7, 13, 15, 1, 3, 4, 12)
KV_COPIES = 16


def nn(a, b):
    return jnp.dot(a, b, preferred_element_type=F32)


def nt(a, b):
    return lax.dot_general(a, b, (((1,), (1,)), ((), ())), preferred_element_type=F32)


def silu(v):
    return v / (1.0 + jnp.exp(-v))


def layer_kernel(
    x_h, ag_h, wq_h, wk_h, wv_h, wf_h, fb_h, wo_h, kv_h, cum_h, len_h, fg_h,
    ids_h, rw_h, sg_h, su_h, sd_h, eg_h, eu_h, ed_h,
    out_ref, nkv_ref,
    x_v, ag_v, w_v, fb_v, wo_v, kv_v, cum_v, len_v, fg_v,
    ids_v, rw_v, sg_v, su_v, sd_v, eg_v, eu_v, ed_v,
    part_s, part_r, mid_a, dsp_s, dsp_r, ret_s, ret_r, fin_s, fin_r, out_a, shared_v,
    lsem, ksem, send_sem, recv_sem,
):
    ep = lax.axis_index("ep")
    tp = lax.axis_index("tp")

    copies = [
        (x_h, x_v), (ag_h, ag_v),
        (wk_h, w_v.at[pl.ds(0, HEAD)]), (wv_h, w_v.at[pl.ds(HEAD, HEAD)]),
        (wq_h, w_v.at[pl.ds(2 * HEAD, HEAD)]), (wf_h, w_v.at[pl.ds(3 * HEAD, N)]),
        (fb_h, fb_v), (cum_h, cum_v), (len_h, len_v),
        (wo_h, wo_v.at[pl.ds(HEAD, HEAD)]), (ids_h, ids_v), (rw_h, rw_v), (fg_h, fg_v),
        (sg_h, sg_v), (su_h, su_v), (sd_h, sd_v), (eg_h, eg_v), (eu_h, eu_v), (ed_h, ed_v),
    ]
    local = [pltpu.make_async_copy(s, d, lsem.at[i]) for i, (s, d) in enumerate(copies)]
    per = ROWS // KV_COPIES
    cached = [
        pltpu.make_async_copy(kv_h.at[pl.ds(i * per, per)], kv_v.at[pl.ds(i * per, per)], ksem.at[i])
        for i in range(KV_COPIES)
    ]
    for c in local[:9]:
        c.start()
    for c in cached:
        c.start()
    for c in local[9:]:
        c.start()

    barrier = pltpu.get_barrier_semaphore()
    for j in range(1, N):
        pl.semaphore_signal(barrier, inc=1, device_id=(ep, lax.rem(tp + j, N)), device_id_type=MESH)
        pl.semaphore_signal(barrier, inc=1, device_id=(lax.rem(ep + j, N), tp), device_id_type=MESH)

    def all_sent(phase, ref):
        pltpu.make_async_remote_copy(
            src_ref=ref, dst_ref=ref, send_sem=send_sem.at[phase], recv_sem=recv_sem.at[phase],
            device_id=(ep, lax.rem(tp + 1, N)), device_id_type=MESH,
        ).wait_send()

    def all_arrived(phase, ref):
        pltpu.make_async_remote_copy(
            src_ref=ref, dst_ref=ref, send_sem=send_sem.at[phase], recv_sem=recv_sem.at[phase],
            device_id=(ep, lax.rem(tp + 1, N)), device_id_type=MESH,
        ).wait_recv()

    def push(phase, src, dst, device):
        pltpu.make_async_remote_copy(
            src_ref=src, dst_ref=dst, send_sem=send_sem.at[phase], recv_sem=recv_sem.at[phase],
            device_id=device, device_id_type=MESH,
        ).start()

    def scatter_tp(phase, src, dst):
        for j in TP_ORDER:
            to = lax.rem(tp + j, N)
            push(phase, src.at[to], dst.at[j - 1], (ep, to))

    def gather_tp(phase, ref):
        for j in TP_ORDER:
            push(phase, ref.at[tp], ref.at[tp], (ep, lax.rem(tp + j, N)))

    def exchange_ep(phase, src, dst):
        for i in EP_ORDER:
            to = lax.rem(ep + i, N)
            push(phase, src.at[:, to], dst.at[:, ep], (to, tp))

    w_v[pl.ds(3 * HEAD + N, HEAD - N)] = jnp.zeros((HEAD - N, WIDTH), BF)
    wo_v[pl.ds(0, HEAD)] = jnp.zeros((HEAD, WIDTH), BF)

    for c in local[:7]:
        c.wait()
    wide = x_v[...].astype(F32)
    factor = lax.rsqrt(jnp.mean(wide * wide, axis=-1, keepdims=True) + NORM_EPS)
    normed = (wide * factor * ag_v[...]).astype(BF)
    res = nt(normed, w_v[...])
    nkv = res[:, :LANES].astype(BF)
    nkv_ref[...] = nkv
    nkv_f = nkv.astype(F32)
    rest = res[:, LANES:]
    lane = lax.broadcasted_iota(jnp.int32, (ROWS, LANES), 1)
    q_f = jnp.where(lane < HEAD, rest, 0.0).astype(BF).astype(F32)
    bias = jnp.sum(
        jnp.where(lax.broadcasted_iota(jnp.int32, (1, N), 1) == tp, fb_v[...], 0.0),
        axis=-1, keepdims=True,
    )
    logit = jnp.sum(jnp.where(lane == HEAD + tp, rest, 0.0), axis=-1, keepdims=True) + bias
    forget = jnp.minimum(logit, 0.0) - jnp.log(1.0 + jnp.exp(-jnp.abs(logit)))
    scaling = HEAD ** (-0.5)
    itself = jnp.sum(q_f * nkv_f, axis=-1, keepdims=True) * scaling

    local[7].wait()
    local[8].wait()
    diag = lax.broadcasted_iota(jnp.int32, (ROWS, ROWS), 0) == lax.broadcasted_iota(
        jnp.int32, (ROWS, ROWS), 1
    )
    length = jnp.sum(
        jnp.where(diag, len_v[...].astype(F32), 0.0), axis=-1, keepdims=True
    ).astype(jnp.int32)
    position = lax.broadcasted_iota(jnp.int32, (8, SPAN), 1)
    row8 = lax.broadcasted_iota(jnp.int32, (8, LANES), 0)
    pieces = []
    for g in range(ROWS // 8):
        here = slice(8 * g, 8 * g + 8)
        for c in cached[8 // per * g : 8 // per * (g + 1)]:
            c.wait()
        q8 = q_f[here]
        scores = jnp.zeros((8, SPAN), F32)
        for p in range(4):
            asked = jnp.concatenate(
                [jnp.where(row8 == 2 * p, q8, 0.0), jnp.where(row8 == 2 * p + 1, q8, 0.0)], axis=1
            ).astype(BF)
            pair = jnp.concatenate([kv_v[8 * g + 2 * p], kv_v[8 * g + 2 * p + 1]], axis=1)
            scores = scores + nt(asked, pair)
        cum = cum_v[pl.ds(8 * g, 8), 0, :]
        len8 = length[here]
        latest = jnp.sum(jnp.where(position == len8 - 1, cum, 0.0), axis=-1, keepdims=True)
        scores = scores * scaling + (latest + forget[here]) - cum
        scores = jnp.where(position < len8, scores, -jnp.inf)
        highest = jnp.maximum(jnp.max(scores, axis=-1, keepdims=True), itself[here])
        earlier = jnp.exp(scores - highest)
        own = jnp.exp(itself[here] - highest)
        denominator = jnp.sum(earlier, axis=-1, keepdims=True) + own
        probs = (earlier / denominator).astype(BF)
        att = (own / denominator).astype(BF).astype(F32) * nkv_f[here]
        for p in range(4):
            pair = jnp.concatenate([kv_v[8 * g + 2 * p], kv_v[8 * g + 2 * p + 1]], axis=1)
            o = nn(probs, pair)
            att = att + jnp.where(row8 == 2 * p, o[:, :LANES], 0.0)
            att = att + jnp.where(row8 == 2 * p + 1, o[:, LANES:], 0.0)
        pieces.append(att)
    attended = jnp.where(lane >= HEAD, jnp.concatenate(pieces, axis=0), 0.0).astype(BF)

    local[9].wait()
    head_part = nn(attended, wo_v[...]).astype(BF)
    for c in range(N):
        part_s[c] = head_part[:, c * LANES : (c + 1) * LANES]
    pl.semaphore_wait(barrier, 2 * (N - 1))
    scatter_tp(0, part_s, part_r)

    for c in local[10:13]:
        c.wait()
    slot = lax.broadcasted_iota(jnp.int32, (ROWS, ROWS), 0)
    target = (slot // 2) * (N // 2) + tp // 2
    member = jnp.zeros((ROWS, ROWS), F32)
    weight = jnp.zeros((ROWS, ROWS), F32)
    for k in range(ids_v.shape[0]):
        hit = ids_v[pl.ds(k, 1), :] == target
        member = jnp.where(hit, 1.0, member)
        weight = weight + jnp.where(hit, rw_v[pl.ds(k, 1), :], 0.0)
    before = (slot < lax.broadcasted_iota(jnp.int32, (ROWS, ROWS), 1)).astype(F32).astype(BF)
    rank = nn(member.astype(BF), before)
    placed = (member > 0.5) & (jnp.abs(rank - (slot % 2).astype(F32)) < 0.5)
    placement = jnp.where(placed, 1.0, 0.0).astype(BF)
    shares = jnp.where(placed, weight, 0.0)
    high = shares.astype(BF)
    low = (shares - high.astype(F32)).astype(BF)
    unit = jnp.where(diag, 1.0, 0.0).astype(BF)
    high = nt(unit, high).astype(BF)
    low = nt(unit, low).astype(BF)

    all_arrived(0, part_r)
    total = part_s[tp].astype(F32)
    for j in range(N - 1):
        total = total + part_r[j].astype(F32)
    own_stream = x_v[:, pl.ds(pl.multiple_of(tp * LANES, LANES), LANES)].astype(F32)
    mid_a[tp] = (own_stream + total).astype(BF)
    gather_tp(1, mid_a)
    all_arrived(1, mid_a.at[pl.ds(0, N - 1)])

    square = jnp.zeros((ROWS, LANES), F32)
    for c in range(N):
        m = mid_a[c].astype(F32)
        square = square + m * m
    factor = lax.rsqrt(jnp.sum(square, axis=-1, keepdims=True) * (1.0 / WIDTH) + NORM_EPS)
    hidden_in = jnp.concatenate(
        [
            (mid_a[c].astype(F32) * factor * fg_v[:, c * LANES : (c + 1) * LANES]).astype(BF)
            for c in range(N)
        ],
        axis=1,
    )
    dispatch = nn(placement, hidden_in).astype(BF)
    dsp_rows = dsp_s.reshape(N, ROWS, LANES)
    for c in range(N):
        dsp_rows[c] = dispatch[:, c * LANES : (c + 1) * LANES]
    exchange_ep(2, dsp_s, dsp_r)

    for c in local[13:16]:
        c.wait()
    shared_hidden = (silu(nt(hidden_in, sg_v[...])) * nt(hidden_in, su_v[...])).astype(BF)
    shared_v[...] = nn(shared_hidden, sd_v[...])
    for c in local[16:]:
        c.wait()

    mine = lax.broadcasted_iota(jnp.int32, (ROWS, LANES), 0) // 2 == ep

    def merged(kept, came):
        kept, came = kept.reshape(N, ROWS, LANES), came.reshape(N, ROWS, LANES)
        return jnp.concatenate(
            [
                jnp.where(mine, kept[c].astype(F32), came[c].astype(F32)).astype(BF)
                for c in range(N)
            ],
            axis=1,
        )

    all_arrived(2, dsp_r.at[pl.ds(0, N - 1)])
    batch = merged(dsp_s, dsp_r)
    hidden = (silu(nn(batch, eg_v[...])) * nn(batch, eu_v[...])).astype(BF)
    served = nn(hidden, ed_v[...]).astype(BF)
    ret_rows = ret_s.reshape(N, ROWS, LANES)
    for c in range(N):
        ret_rows[c] = served[:, c * LANES : (c + 1) * LANES]
    exchange_ep(3, ret_s, ret_r)
    all_arrived(3, ret_r.at[pl.ds(0, N - 1)])

    returned = merged(ret_s, ret_r)
    mixed = (shared_v[...] + (nn(high, returned) + nn(low, returned))).astype(BF)
    for c in range(N):
        fin_s[c] = mixed[:, c * LANES : (c + 1) * LANES]
    scatter_tp(4, fin_s, fin_r)
    all_arrived(4, fin_r)
    total = mid_a[tp].astype(F32) + fin_s[tp].astype(F32)
    for j in range(N - 1):
        total = total + fin_r[j].astype(F32)
    out_a[tp] = total.astype(BF)
    gather_tp(5, out_a)
    all_arrived(5, out_a.at[pl.ds(0, N - 1)])
    for c in range(N):
        out_ref[:, c * LANES : (c + 1) * LANES] = out_a[c]

    for phase in range(6):
        all_sent(phase, part_r)


def body(
    layer_in, attn_gain, query_weight, key_weight, value_weight, forget_weight, forget_bias,
    out_weight, kv_cache, cum_gates, lengths, ffn_gain, route_ids, route_weights,
    shared_gate, shared_up, shared_down, expert_gate, expert_up, expert_down,
):
    operands = (
        layer_in, attn_gain.reshape(1, -1), query_weight.T, key_weight.T, value_weight.T,
        forget_weight.T, forget_bias.reshape(1, -1), out_weight, kv_cache[:, 0], cum_gates,
        lengths.reshape(1, -1), ffn_gain.reshape(1, -1), route_ids.T, route_weights.T,
        shared_gate.T, shared_up.T, shared_down, expert_gate[0], expert_up[0], expert_down[0],
    )
    picks = route_ids.shape[1]
    block = (N, ROWS, LANES)
    paired = (N, N, 2, LANES)
    layer_out, new_kv = pl.pallas_call(
        layer_kernel,
        out_shape=(
            jax.ShapeDtypeStruct((ROWS, WIDTH), BF),
            jax.ShapeDtypeStruct((ROWS, LANES), BF),
        ),
        in_specs=[pl.BlockSpec(memory_space=pltpu.HBM)] * len(operands),
        out_specs=[pl.BlockSpec(memory_space=pltpu.VMEM)] * 2,
        scratch_shapes=[
            pltpu.VMEM((ROWS, WIDTH), BF),
            pltpu.VMEM((1, WIDTH), F32),
            pltpu.VMEM((4 * HEAD, WIDTH), BF),
            pltpu.VMEM((1, N), F32),
            pltpu.VMEM((2 * HEAD, WIDTH), BF),
            pltpu.VMEM((ROWS, SPAN, LANES), BF),
            pltpu.VMEM((ROWS, 1, SPAN), F32),
            pltpu.VMEM((1, ROWS), jnp.int32),
            pltpu.VMEM((1, WIDTH), F32),
            pltpu.VMEM((picks, ROWS), jnp.int32),
            pltpu.VMEM((picks, ROWS), F32),
            pltpu.VMEM((ROWS, WIDTH), BF),
            pltpu.VMEM((ROWS, WIDTH), BF),
            pltpu.VMEM((ROWS, WIDTH), BF),
            pltpu.VMEM((WIDTH, 4 * HEAD), BF),
            pltpu.VMEM((WIDTH, 4 * HEAD), BF),
            pltpu.VMEM((4 * HEAD, WIDTH), BF),
            pltpu.VMEM(block, BF),
            pltpu.VMEM((N - 1, ROWS, LANES), BF),
            pltpu.VMEM(block, BF),
            pltpu.VMEM(paired, BF),
            pltpu.VMEM(paired, BF),
            pltpu.VMEM(paired, BF),
            pltpu.VMEM(paired, BF),
            pltpu.VMEM(block, BF),
            pltpu.VMEM((N - 1, ROWS, LANES), BF),
            pltpu.VMEM(block, BF),
            pltpu.VMEM((ROWS, WIDTH), F32),
            pltpu.SemaphoreType.DMA((len(operands) - 1,)),
            pltpu.SemaphoreType.DMA((KV_COPIES,)),
            pltpu.SemaphoreType.DMA((6,)),
            pltpu.SemaphoreType.DMA((6,)),
        ],
        compiler_params=pltpu.CompilerParams(collective_id=0, has_side_effects=True),
        name="decode_layer",
    )(*operands)
    return (layer_out, new_kv[:, None, :])


def solution(mesh):
    placed = (
        P("ep", None), P(), P(None, "tp"), P(None, "tp"), P(None, "tp"), P(), P(), P("tp", None),
        P("ep", "tp", None, None), P("ep", "tp", None), P("ep"), P(), P("ep", None),
        P("ep", None), P(None, "tp"), P(None, "tp"), P("tp", None), P(("ep", "tp"), None, None),
        P(("ep", "tp"), None, None), P(("ep", "tp"), None, None),
    )
    return jax.shard_map(
        body,
        mesh=mesh,
        in_specs=placed,
        out_specs=(P("ep", None), P("ep", "tp", None)),
        check_vma=False,
    )
```

time: 122 us -> 52.2 us (0.43)
  Pallas kernels: 0 us -> 48.5 us
  blocking collectives: 31.4 us -> 0 us
  starting transfers between devices: 27.7 us -> 0 us
  waiting for transfers between devices: 25.3 us -> 0 us
  matrix products: 17.3 us -> 0 us
  other arithmetic: 9.49 us -> 0 us
  local copies, waits for them, and re-layouts: 8.9 us -> 2.86 us
    pallas_call x0 -> x1, Pallas kernels: none -> 48.5 us  [body(): pl.pallas_call(layer_kernel, out_shape=(jax.ShapeDtypeStruct((ROWS, WIDTH...]
    all_gather x2 -> x0, blocking collectives: 31.4 us -> none  [the longest x1 16.6 us: in_one_piece(): filled, at, outs = (lax.all_gather(both, axis, axis=dim, tiled=True), 0, [])]
    all_to_all x4 -> x0, starting transfers between devices: 27.7 us -> none  [the longest x2 17.4 us: summed_on_arrival(): lax.all_to_all(tiles, axis, split_axis=0, concat_axis=0, tiled=True)]
    all_to_all x4 -> x0, waiting for transfers between devices: 25.3 us -> none  [the longest x2 14 us: summed_on_arrival(): lax.all_to_all(tiles, axis, split_axis=0, concat_axis=0, tiled=True)]
    dot_general x14 -> x0, matrix products: 17.3 us -> none  [the longest x1 5.63 us: attend(): jnp.einsum('shd,shld->shl', queries, cached_keys, preferred_element_type=...]
    reduce_sum x7 -> x0, other arithmetic: 4.48 us -> none  [the longest x1 1.76 us: attend(): latest = jnp.sum(jnp.where(at_last, cum_block, 0.0), axis=-1)]
    reshape x4 -> x0, local copies, waits for them, and re-layouts: 3.24 us -> none  [the longest x2 1.52 us: cut_along(): return jnp.moveaxis(shard.reshape(*before, peers, -1, *after), dim, 0)]
    dynamic_slice x1 -> x0, local copies, waits for them, and re-layouts: 1.39 us -> none  [body(): lax.dynamic_slice_in_dim(gate_logits, first_head, heads_here, 1)]
  transfers between devices with their start and end apart: 4 -> 0, of which waited for: 4 -> 0; matrix products, arithmetic and copies ran while one was open for 5% -> 0% of each run, Pallas kernels for 0% -> 0%
where the time goes in v1:
time: 52.2 us; the launch traced here: 52 us
  Pallas kernels  48.5 us (93%)
  local copies, waits for them, and re-layouts  2.86 us (5%)
  between operations  0.65 us (1%)
    pallas_call x1, Pallas kernels, body(): pl.pallas_call(layer_kernel, out_shape=(jax.ShapeDtypeStruct((ROWS, WIDTH...  48.5 us
    unnamed x2, local copies, waits for them, and re-layouts  2.86 us

profile of v1, /device:TPU:1, one launch (start us, length us, event | category | flops | bytes accessed | tf_op | source)
XLA Modules:
  0.0 52.0 jit_solution(888123563233904151)
XLA Ops:
  0.6 48.5 %decode_layer.1 = (bf16[32,2048]{1,0:T(8,128)(2,1)}, bf16[32,128]{1,0:T(8,128)(2,1)}) custom-call(bf16[32,2048]{1,0:T(8,128)(2,1)} %x_h.1, f32[1,2048]{1,0:T(1,128)} %bitcast.27, bf16[64,2048]{1,0:T(8,128)(2,1)} %bitcast.21, bf16[64,2048]{1,0:T(8,128)(2,1)} %bitcast.22, bf16[64,2048]{1,0:T(8,128)(2,1)} %bitcast.23, bf16[16,2048]{1,0:T(8,128)(2,1)} %bitcast.26, ...), custom_call_target="tpu_custom_call" | custom-call | tf_op jit(solution)/shard_map/decode_layer/pallas_call | solution.py:288
  49.2 1.6 %copy.24 = bf16[32,2048]{1,0:T(8,128)(2,1)} copy(bf16[32,2048]{1,0:T(8,128)(2,1)} %get-tuple-element.8) | data formatting | bytes 262144
  50.7 1.3 %copy.25 = bf16[32,1,128]{2,0,1:T(8,128)(2,1)} copy(bf16[32,1,128]{2,0,1:T(8,128)(2,1)} %bitcast.29) | data formatting | bytes 16384

commit v2 on v1

--- a/solution.py
+++ b/solution.py
@@ -16,7 +16,6 @@
 SPAN = 1024
 HEAD = 64
 TP_ORDER = (8, 9, 7, 6, 10, 11, 5, 4, 12, 13, 3, 2, 14, 15, 1)
-EP_ORDER = (10, 6, 14, 9, 11, 2, 8, 5, 7, 13, 15, 1, 3, 4, 12)
 KV_COPIES = 16
 
 
@@ -38,8 +37,8 @@
     out_ref, nkv_ref,
     x_v, ag_v, w_v, fb_v, wo_v, kv_v, cum_v, len_v, fg_v,
     ids_v, rw_v, sg_v, su_v, sd_v, eg_v, eu_v, ed_v,
-    part_s, part_r, mid_a, dsp_s, dsp_r, ret_s, ret_r, fin_s, fin_r, out_a, shared_v,
-    lsem, ksem, send_sem, recv_sem,
+    part_s, part_r, mid_a, dsp_s, dsp_r, ret_s, ret_r, fin_s, fin_r, out_a,
+    lsem, ksem, send_sem, recv_sem, ready,
 ):
     ep = lax.axis_index("ep")
     tp = lax.axis_index("tp")
@@ -97,10 +96,18 @@
         for j in TP_ORDER:
             push(phase, ref.at[tp], ref.at[tp], (ep, lax.rem(tp + j, N)))
 
-    def exchange_ep(phase, src, dst):
-        for i in EP_ORDER:
-            to = lax.rem(ep + i, N)
-            push(phase, src.at[:, to], dst.at[:, ep], (to, tp))
+    def everywhere(phase, pick, dst):
+        def to_ep(i, carry):
+            far = lax.rem(ep + i, N)
+            for j in (0,) + TP_ORDER:
+                to = lax.rem(tp + j, N)
+                push(phase, pick(far, to), dst, (far, to))
+            return carry
+
+        lax.fori_loop(1, N, to_ep, 0)
+        for j in TP_ORDER:
+            to = lax.rem(tp + j, N)
+            push(phase, pick(ep, to), dst, (ep, to))
 
     w_v[pl.ds(3 * HEAD + N, HEAD - N)] = jnp.zeros((HEAD - N, WIDTH), BF)
     wo_v[pl.ds(0, HEAD)] = jnp.zeros((HEAD, WIDTH), BF)
@@ -173,19 +180,29 @@
     for c in range(N):
         part_s[c] = head_part[:, c * LANES : (c + 1) * LANES]
     pl.semaphore_wait(barrier, 2 * (N - 1))
+    for j in range(1, N):
+        pl.semaphore_signal(
+            ready, inc=1, device_id=(lax.rem(ep + j, N), tp), device_id_type=MESH
+        )
     scatter_tp(0, part_s, part_r)
 
     for c in local[10:13]:
         c.wait()
-    slot = lax.broadcasted_iota(jnp.int32, (ROWS, ROWS), 0)
-    target = (slot // 2) * (N // 2) + tp // 2
-    member = jnp.zeros((ROWS, ROWS), F32)
-    weight = jnp.zeros((ROWS, ROWS), F32)
+    experts = N * N // 2
+    slot = lax.broadcasted_iota(jnp.int32, (2 * experts, ROWS), 0)
+    target = slot // 2
+    member = jnp.zeros(slot.shape, F32)
+    weight = jnp.zeros(slot.shape, F32)
     for k in range(ids_v.shape[0]):
         hit = ids_v[pl.ds(k, 1), :] == target
         member = jnp.where(hit, 1.0, member)
         weight = weight + jnp.where(hit, rw_v[pl.ds(k, 1), :], 0.0)
-    before = (slot < lax.broadcasted_iota(jnp.int32, (ROWS, ROWS), 1)).astype(F32).astype(BF)
+    before = jnp.where(
+        lax.broadcasted_iota(jnp.int32, (ROWS, ROWS), 0)
+        < lax.broadcasted_iota(jnp.int32, (ROWS, ROWS), 1),
+        1.0,
+        0.0,
+    ).astype(BF)
     rank = nn(member.astype(BF), before)
     placed = (member > 0.5) & (jnp.abs(rank - (slot % 2).astype(F32)) < 0.5)
     placement = jnp.where(placed, 1.0, 0.0).astype(BF)
@@ -201,74 +218,68 @@
     for j in range(N - 1):
         total = total + part_r[j].astype(F32)
     own_stream = x_v[:, pl.ds(pl.multiple_of(tp * LANES, LANES), LANES)].astype(F32)
-    mid_a[tp] = (own_stream + total).astype(BF)
+    middle = (own_stream + total).astype(BF)
+    mid_a[tp] = middle
+    dsp_s.reshape(2 * experts, LANES)[...] = nn(placement, middle).astype(BF)
+    pl.semaphore_wait(ready, N - 1)
+    everywhere(2, lambda e, t: dsp_s.at[e * (N // 2) + t // 2], dsp_r.at[tp, ep])
+    dsp_r[tp, ep] = dsp_s[ep * (N // 2) + tp // 2]
     gather_tp(1, mid_a)
-    all_arrived(1, mid_a.at[pl.ds(0, N - 1)])
-
-    square = jnp.zeros((ROWS, LANES), F32)
-    for c in range(N):
-        m = mid_a[c].astype(F32)
-        square = square + m * m
-    factor = lax.rsqrt(jnp.sum(square, axis=-1, keepdims=True) * (1.0 / WIDTH) + NORM_EPS)
-    hidden_in = jnp.concatenate(
-        [
-            (mid_a[c].astype(F32) * factor * fg_v[:, c * LANES : (c + 1) * LANES]).astype(BF)
-            for c in range(N)
-        ],
-        axis=1,
-    )
-    dispatch = nn(placement, hidden_in).astype(BF)
-    dsp_rows = dsp_s.reshape(N, ROWS, LANES)
-    for c in range(N):
-        dsp_rows[c] = dispatch[:, c * LANES : (c + 1) * LANES]
-    exchange_ep(2, dsp_s, dsp_r)
-
-    for c in local[13:16]:
-        c.wait()
-    shared_hidden = (silu(nt(hidden_in, sg_v[...])) * nt(hidden_in, su_v[...])).astype(BF)
-    shared_v[...] = nn(shared_hidden, sd_v[...])
-    for c in local[16:]:
-        c.wait()
-
-    mine = lax.broadcasted_iota(jnp.int32, (ROWS, LANES), 0) // 2 == ep
-
-    def merged(kept, came):
-        kept, came = kept.reshape(N, ROWS, LANES), came.reshape(N, ROWS, LANES)
+
+    def normalised(blocks):
+        square = jnp.zeros((ROWS, LANES), F32)
+        for c in range(N):
+            m = blocks[c].astype(F32)
+            square = square + m * m
+        factor = lax.rsqrt(jnp.sum(square, axis=-1, keepdims=True) * (1.0 / WIDTH) + NORM_EPS)
         return jnp.concatenate(
             [
-                jnp.where(mine, kept[c].astype(F32), came[c].astype(F32)).astype(BF)
+                (blocks[c].astype(F32) * factor * fg_v[:, c * LANES : (c + 1) * LANES]).astype(BF)
                 for c in range(N)
             ],
             axis=1,
         )
 
-    all_arrived(2, dsp_r.at[pl.ds(0, N - 1)])
-    batch = merged(dsp_s, dsp_r)
+    for c in local[13:]:
+        c.wait()
+    all_arrived(2, dsp_r.reshape(N * N, 2, LANES).at[pl.ds(0, N * N - 1)])
+    batch = normalised(dsp_r.reshape(N, ROWS, LANES))
     hidden = (silu(nn(batch, eg_v[...])) * nn(batch, eu_v[...])).astype(BF)
     served = nn(hidden, ed_v[...]).astype(BF)
     ret_rows = ret_s.reshape(N, ROWS, LANES)
     for c in range(N):
         ret_rows[c] = served[:, c * LANES : (c + 1) * LANES]
-    exchange_ep(3, ret_s, ret_r)
-    all_arrived(3, ret_r.at[pl.ds(0, N - 1)])
-
-    returned = merged(ret_s, ret_r)
-    mixed = (shared_v[...] + (nn(high, returned) + nn(low, returned))).astype(BF)
+    mine = ep * (N // 2) + tp // 2
+    everywhere(3, lambda e, t: ret_s.at[t, e], ret_r.at[lax.rem(tp, 2), mine])
+    ret_r[lax.rem(tp, 2), mine] = ret_s[tp, ep]
+
+    all_arrived(1, mid_a.at[pl.ds(0, N - 1)])
+    hidden_in = normalised(mid_a)
+    shared_hidden = (silu(nt(hidden_in, sg_v[...])) * nt(hidden_in, su_v[...])).astype(BF)
+    mixed = nn(shared_hidden, sd_v[...]).astype(BF)
     for c in range(N):
         fin_s[c] = mixed[:, c * LANES : (c + 1) * LANES]
     scatter_tp(4, fin_s, fin_r)
+
     all_arrived(4, fin_r)
     total = mid_a[tp].astype(F32) + fin_s[tp].astype(F32)
     for j in range(N - 1):
         total = total + fin_r[j].astype(F32)
+    all_arrived(3, ret_r.reshape(N * N, 2, LANES).at[pl.ds(0, N * N - 1)])
+    ret_half = ret_r.reshape(2, 2 * experts, LANES)
+    for c in range(2):
+        returned = ret_half[c]
+        total = total + nn(high, returned) + nn(low, returned)
     out_a[tp] = total.astype(BF)
     gather_tp(5, out_a)
     all_arrived(5, out_a.at[pl.ds(0, N - 1)])
     for c in range(N):
         out_ref[:, c * LANES : (c + 1) * LANES] = out_a[c]
 
-    for phase in range(6):
+    for phase in (0, 1, 4, 5):
         all_sent(phase, part_r)
+    for phase in (2, 3):
+        all_sent(phase, dsp_r.reshape(N * N, 2, LANES).at[pl.ds(0, N * N - 1)])
 
 
 def body(
@@ -284,7 +295,6 @@
     )
     picks = route_ids.shape[1]
     block = (N, ROWS, LANES)
-    paired = (N, N, 2, LANES)
     layer_out, new_kv = pl.pallas_call(
         layer_kernel,
         out_shape=(
@@ -314,18 +324,18 @@
             pltpu.VMEM(block, BF),
             pltpu.VMEM((N - 1, ROWS, LANES), BF),
             pltpu.VMEM(block, BF),
-            pltpu.VMEM(paired, BF),
-            pltpu.VMEM(paired, BF),
-            pltpu.VMEM(paired, BF),
-            pltpu.VMEM(paired, BF),
+            pltpu.VMEM((N * N // 2, 2, LANES), BF),
+            pltpu.VMEM((N, N, 2, LANES), BF),
+            pltpu.VMEM((N, N, 2, LANES), BF),
+            pltpu.VMEM((2, N * N // 2, 2, LANES), BF),
             pltpu.VMEM(block, BF),
             pltpu.VMEM((N - 1, ROWS, LANES), BF),
             pltpu.VMEM(block, BF),
-            pltpu.VMEM((ROWS, WIDTH), F32),
             pltpu.SemaphoreType.DMA((len(operands) - 1,)),
             pltpu.SemaphoreType.DMA((KV_COPIES,)),
             pltpu.SemaphoreType.DMA((6,)),
             pltpu.SemaphoreType.DMA((6,)),
+            pltpu.SemaphoreType.REGULAR,
         ],
         compiler_params=pltpu.CompilerParams(collective_id=0, has_side_effects=True),
         name="decode_layer",

time: 52.2 us -> 48.9 us (0.937)
  Pallas kernels: 48.5 us -> 45.2 us
    pallas_call x1, Pallas kernels: 48.5 us -> 45.2 us  [body(): pl.pallas_call(layer_kernel, out_shape=(jax.ShapeDtypeStruct((ROWS, WIDTH...]
where the time goes in v2:
time: 48.9 us; the launch traced here: 48.7 us
  Pallas kernels  45.2 us (92%)
  local copies, waits for them, and re-layouts  2.86 us (6%)
  between operations  0.65 us (1%)
    pallas_call x1, Pallas kernels, body(): pl.pallas_call(layer_kernel, out_shape=(jax.ShapeDtypeStruct((ROWS, WIDTH...  45.2 us
    unnamed x2, local copies, waits for them, and re-layouts  2.86 us

profile of v2, /device:TPU:1, one launch (start us, length us, event | category | flops | bytes accessed | tf_op | source)
XLA Modules:
  0.0 48.7 jit_solution(15087302488277581232)
XLA Ops:
  0.6 45.2 %decode_layer.1 = (bf16[32,2048]{1,0:T(8,128)(2,1)}, bf16[32,128]{1,0:T(8,128)(2,1)}) custom-call(bf16[32,2048]{1,0:T(8,128)(2,1)} %x_h.1, f32[1,2048]{1,0:T(1,128)} %bitcast.27, bf16[64,2048]{1,0:T(8,128)(2,1)} %bitcast.21, bf16[64,2048]{1,0:T(8,128)(2,1)} %bitcast.22, bf16[64,2048]{1,0:T(8,128)(2,1)} %bitcast.23, bf16[16,2048]{1,0:T(8,128)(2,1)} %bitcast.26, ...), custom_call_target="tpu_custom_call" | custom-call | tf_op jit(solution)/shard_map/decode_layer/pallas_call | solution.py:298
  45.9 1.6 %copy.24 = bf16[32,2048]{1,0:T(8,128)(2,1)} copy(bf16[32,2048]{1,0:T(8,128)(2,1)} %get-tuple-element.8) | data formatting | bytes 262144
  47.4 1.3 %copy.25 = bf16[32,1,128]{2,0,1:T(8,128)(2,1)} copy(bf16[32,1,128]{2,0,1:T(8,128)(2,1)} %bitcast.29) | data formatting | bytes 16384

commit v3 on v2

--- a/solution.py
+++ b/solution.py
@@ -298,8 +298,8 @@
     layer_out, new_kv = pl.pallas_call(
         layer_kernel,
         out_shape=(
-            jax.ShapeDtypeStruct((ROWS, WIDTH), BF),
-            jax.ShapeDtypeStruct((ROWS, LANES), BF),
+            pltpu.VMEM((ROWS, WIDTH), BF),
+            pltpu.VMEM((ROWS, LANES), BF),
         ),
         in_specs=[pl.BlockSpec(memory_space=pltpu.HBM)] * len(operands),
         out_specs=[pl.BlockSpec(memory_space=pltpu.VMEM)] * 2,

time: 48.9 us -> 46.4 us (0.949)
  local copies, waits for them, and re-layouts: 2.86 us -> 1.26 us
  Pallas kernels: 45.2 us -> 44.4 us
    unnamed x2, local copies, waits for them, and re-layouts: 2.86 us -> 1.26 us
    pallas_call x1, Pallas kernels: 45.2 us -> 44.4 us  [body(): pl.pallas_call(layer_kernel, out_shape=(pltpu.VMEM((ROWS, WIDTH), BF), pl...]
where the time goes in v3:
time: 46.4 us; the launch traced here: 46.3 us
  Pallas kernels  44.4 us (96%)
  local copies, waits for them, and re-layouts  1.26 us (3%)
  between operations  0.65 us (1%)
    pallas_call x1, Pallas kernels, body(): pl.pallas_call(layer_kernel, out_shape=(pltpu.VMEM((ROWS, WIDTH), BF), pl...  44.4 us
    unnamed x2, local copies, waits for them, and re-layouts  1.26 us

profile of v3, /device:TPU:1, one launch (start us, length us, event | category | flops | bytes accessed | tf_op | source)
XLA Modules:
  0.0 46.3 jit_solution(835498885972118698)
XLA Ops:
  0.6 44.4 %decode_layer.1 = (bf16[32,2048]{1,0:T(8,128)(2,1)S(1)}, bf16[32,128]{1,0:T(8,128)(2,1)S(1)}) custom-call(bf16[32,2048]{1,0:T(8,128)(2,1)} %x_h.1, f32[1,2048]{1,0:T(1,128)} %bitcast.28, bf16[64,2048]{1,0:T(8,128)(2,1)} %bitcast.22, bf16[64,2048]{1,0:T(8,128)(2,1)} %bitcast.23, bf16[64,2048]{1,0:T(8,128)(2,1)} %bitcast.24, bf16[16,2048]{1,0:T(8,128)(2,1)} %bitcast.27, ...), custom_call_target="tpu_custom_call" | custom-call | tf_op jit(solution)/shard_map/decode_layer/pallas_call | solution.py:298
  45.0 0.7 %copy.24 = bf16[32,2048]{1,0:T(8,128)(2,1)} copy(bf16[32,2048]{1,0:T(8,128)(2,1)S(1)} %get-tuple-element.6) | data formatting | bytes 262144
  45.7 0.6 %copy.25 = bf16[32,1,128]{2,0,1:T(8,128)(2,1)} copy(bf16[32,1,128]{2,0,1:T(8,128)(2,1)S(1)} %bitcast.17) | data formatting | bytes 16384
